TPU v7x, 128 devices: a whole 4x4x4 slice. The times are simulated.
128 devices in a mesh: sp: 32 (over z, y, core), tp: 4 (over x).
Axes of the slice: x: 4, y: 4, z: 4, core: 2. Of those that a mesh axis runs over, the one named last changes fastest.
Arguments:
- activations: bfloat16 [2, 1024, 1024], P(None, 'sp', 'tp'), may hold values from -6 to 6
- norm_gain: float32 [4, 1024], replicated, may hold values from 0.1 to 1.9
- in_weight: bfloat16 [4, 1024, 512], P(None, 'sp', 'tp'), may hold values from -0.1875 to 0.1875
- out_weight: bfloat16 [4, 512, 1024], P(None, 'tp', 'sp'), may hold values from -0.25 to 0.25
- mixing: bfloat16 [4, 4, 128, 128], P(None, 'tp', 'sp'), may hold values from -0.5 to 0.5
- pool_scale: float32 [4, 512], P(None, 'tp'), may hold values from 0.1 to 1.9
Outputs:
- result: bfloat16 [2, 1024, 1024], P(None, 'sp', 'tp')
All inputs are finite; a program needn't handle non-finite values.
Results may differ from a plain program's by a relative error of at most 0.03.
Values may be sent and summed in bfloat16 or wider, within the bound.
A program may use at most 64 MiB of HBM per device.

v0:
```python
import functools

import jax
import jax.numpy as jnp
from jax import lax
from jax.experimental import pallas as pl
from jax.experimental.pallas import tpu as pltpu
from jax.sharding import PartitionSpec as P

F32, BF16 = jnp.float32, jnp.bfloat16
MINOR = 2


def kernel(sp_size, halo, act_in, gain_in, w_in, w_out, mix, scale_in, out, act, gain, scale, g_in, g_out, g_mix, st0, *rest):
    layers, in_rows, cols = w_in.shape
    seqs, toks, blk = act.shape
    width = gain.shape[1]
    major = sp_size // MINOR
    bufs = [rest[5 * l : 5 * l + 5] for l in range(layers)]
    (s_z, r_z, s_y, r_y, s_own, s_act, r_act, s_ar, r_ar) = rest[5 * layers :]
    sp, tp = lax.axis_index("sp"), lax.axis_index("tp")
    a, b = sp // MINOR, sp % MINOR
    q, h = tp // 2, tp % 2
    h0 = layers * halo

    def near(x):
        return lax.rem(x + sp_size, sp_size)

    def remote(src, dst, ss, rs, sp_to, tp_to):
        return pltpu.make_async_remote_copy(
            src_ref=src, dst_ref=dst, send_sem=ss, recv_sem=rs,
            device_id={"sp": sp_to, "tp": tp_to}, device_id_type=pl.DeviceIdType.MESH,
        )

    tp_peers = [lax.rem(tp + k, 4) for k in range(1, 4)]
    z_peers = [lax.rem(a + k, major) * MINOR + b for k in range(1, major)]
    y_peer = a * MINOR + (1 - b)

    owns = [(w_in, g_in), (w_out, g_out), (mix, g_mix)]
    placed = [(act_in, act), (w_in, g_in.at[:, sp]), (w_out, g_out.at[:, sp]), (mix, g_mix.at[:, sp])]
    placed += [(gain_in, gain), (scale_in, scale)]
    own_copies = [pltpu.make_async_copy(src, dst, s_own.at[i]) for i, (src, dst) in enumerate(placed)]

    barrier = pltpu.get_barrier_semaphore()
    everyone = [(sp, t) for t in tp_peers] + [(p, tp) for p in z_peers]
    everyone += [(y_peer, tp), (near(sp - 1), tp), (near(sp + 1), tp)]
    for s_to, t_to in everyone:
        pl.semaphore_signal(
            barrier, inc=1, device_id={"sp": s_to, "tp": t_to}, device_id_type=pl.DeviceIdType.MESH
        )
    for c in own_copies:
        c.start()
    for c in own_copies:
        c.wait()
    pl.semaphore_wait(barrier, len(everyone))

    pending = []

    def z_send(kind, l):
        src, dst = owns[kind]
        for k in range(1, major):
            c = remote(dst.at[l, sp], dst.at[l, sp], s_z.at[kind, l, k], r_z.at[kind, l, k], z_peers[k - 1], tp)
            c.start()
            pending.append(c)

    def y_send(kind, l, k):
        src, dst = owns[kind]
        origin = lax.rem(a - k + major, major) * MINOR + b
        c = remote(dst.at[l, origin], dst.at[l, origin], s_y.at[kind, l, k], r_y.at[kind, l, k], y_peer, tp)
        c.start()
        pending.append(c)

    def forward(kind, l):
        src, dst = owns[kind]
        for k in range(1, major):
            origin = lax.rem(a - k + major, major) * MINOR + b
            remote(dst.at[l, origin], dst.at[l, origin], s_z.at[kind, l, k], r_z.at[kind, l, k], y_peer, tp).wait_recv()
            y_send(kind, l, k)

    def arrived(kind, l):
        src, dst = owns[kind]
        for k in range(major):
            origin = lax.rem(a - k + major, major) * MINOR + (1 - b)
            remote(dst.at[l, origin], dst.at[l, origin], s_y.at[kind, l, k], r_y.at[kind, l, k], y_peer, tp).wait_recv()

    def launch(kind, l):
        z_send(kind, l)
        y_send(kind, l, 0)

    has_left, has_right = sp > 0, sp < sp_size - 1
    left_rows, own_rows, right_rows = pl.ds(0, h0), pl.ds(h0, toks), pl.ds(h0 + toks, h0)
    to_right = remote(
        act.at[:, pl.ds(toks - h0, h0)], st0.at[h, q, :, left_rows], s_act.at[0, 0], r_act.at[0, 0], near(sp + 1), tp
    )
    to_left = remote(
        act.at[:, pl.ds(0, h0)], st0.at[h, q, :, right_rows], s_act.at[1, 0], r_act.at[1, 0], near(sp - 1), tp
    )
    pl.when(has_right)(to_right.start)
    pl.when(has_left)(to_left.start)
    launch(0, 0)
    own_out = []
    for k in range(1, 4):
        c = remote(act, st0.at[h, q, :, own_rows], s_act.at[2, k], r_act.at[2, k], sp, tp_peers[k - 1])
        c.start()
        own_out.append(c)
    launch(2, 0)
    launch(1, 0)
    st0[h, q, :, h0 : h0 + toks, :] = act[...]

    def spread(side, rows):
        return [
            remote(st0.at[h, q, :, rows], st0.at[h, q, :, rows], s_act.at[side, k], r_act.at[side, k], sp, tp_peers[k - 1])
            for k in range(1, 4)
        ]

    def take_side(side, rows, incoming):
        def yes():
            incoming.wait_recv()
            for c in spread(side, rows):
                c.start()

        return yes

    def blank(rows):
        def fill():
            st0[:, :, :, rows, :] = jnp.zeros((2, 2, seqs, h0, blk), BF16)

        return fill

    pl.when(has_left)(take_side(0, left_rows, to_right))
    pl.when(has_right)(take_side(1, right_rows, to_left))
    pl.when(jnp.logical_not(has_left))(blank(left_rows))
    pl.when(jnp.logical_not(has_right))(blank(right_rows))
    forward(0, 0)
    forward(2, 0)
    forward(1, 0)
    if layers > 1:
        launch(0, 1)
        launch(2, 1)
        launch(1, 1)
    for c in own_out:
        c.wait()

    def finish_side(side, rows):
        def yes():
            for c in spread(side, rows):
                c.wait()

        return yes

    pl.when(has_left)(finish_side(0, left_rows))
    pl.when(has_right)(finish_side(1, right_rows))
    arrived(0, 0)

    seq_len = toks * sp_size
    half_window = lax.shift_left(jnp.int32(1), tp)

    def centring(l, n_in, n_out):
        base = sp * toks - (layers - l) * halo
        pos = base + halo + lax.broadcasted_iota(jnp.int32, (n_out, n_in), 0)
        src = base + lax.broadcasted_iota(jnp.int32, (n_out, n_in), 1)
        low = jnp.maximum(pos - half_window, 0)
        high = jnp.minimum(pos + half_window, seq_len)
        band = jnp.where((src >= low) & (src < high), 1.0, 0.0).astype(BF16)
        col = base + halo + lax.broadcasted_iota(jnp.int32, (n_out, 1), 0)
        count = jnp.minimum(col + half_window, seq_len) - jnp.maximum(col - half_window, 0)
        return band, 1.0 / jnp.maximum(count, 1).astype(F32)

    def state_of(l, s, hh, qq):
        return st0[hh, qq, s] if l == 0 else bufs[l - 1][4][s, hh, qq]

    def pooled_of(l, s):
        xs = [state_of(l, s, t % 2, t // 2).astype(F32) for t in range(4)]
        total = sum(jnp.sum(x * x, axis=-1, keepdims=True) for x in xs)
        inv = lax.rsqrt(total * (1.0 / width) + 1e-06)
        weight = g_in[l].reshape(width, cols)
        acc = None
        for t in range(4):
            normed = (xs[t] * inv * gain[l : l + 1, t * blk : (t + 1) * blk]).astype(BF16)
            term = jnp.dot(normed, weight[t * blk : (t + 1) * blk], preferred_element_type=F32)
            acc = term if acc is None else acc + term
        return acc.astype(BF16)

    def out_partial(l, s, pooled, band, inv_count):
        part = bufs[l][0]
        n_out = band.shape[0]
        sums = jnp.dot(band, pooled, preferred_element_type=F32)
        centred = (sums * inv_count - pooled.astype(F32)[halo : halo + n_out]).astype(BF16)
        mixing = g_mix[l].astype(F32).reshape(cols, cols).astype(BF16)
        mixed = jnp.dot(centred, mixing, preferred_element_type=F32)
        joined = (mixed * scale[l : l + 1, :]).astype(BF16)
        per = sp_size // 4
        for t in range(4):
            weight = jnp.concatenate([g_out[l, j] for j in range(t * per, (t + 1) * per)], axis=1)
            part[s, t % 2, t // 2] = jnp.dot(joined, weight, preferred_element_type=F32).astype(BF16)

    core_peer, far_peer = q * 2 + (1 - h), (1 - q) * 2 + h

    for l in range(layers):
        last = l == layers - 1
        n_in = toks + 2 * (layers - l) * halo
        n_out = n_in - 2 * halo
        part, r1, hf, r2, nxt = bufs[l]
        band, inv_count = centring(l, n_in, n_out)

        def stage(i, s, src, dst, peer):
            c = remote(src, dst, s_ar.at[i, l, s], r_ar.at[i, l, s], sp, peer)
            c.start()
            pending.append(c)
            return c

        first, second, third = [], [], []
        for s in range(seqs):
            if l > 0:
                gathers[s].wait_recv()
            pooled = pooled_of(l, s)
            if s == 0:
                arrived(2, l)
                arrived(1, l)
            out_partial(l, s, pooled, band, inv_count)
            first.append(stage(0, s, part.at[s, 1 - h], r1.at[s], core_peer))
        if not last:
            forward(0, l + 1)
        for s in range(seqs):
            first[s].wait_recv()
            hf[s] = (part[s, h].astype(F32) + r1[s].astype(F32)).astype(BF16)
            if last:
                second.append(stage(1, s, hf.at[s, 1 - q], r2.at[s, 0], far_peer))
            else:
                second.append(stage(1, s, hf.at[s], r2.at[s], far_peer))
        if not last:
            forward(2, l + 1)
            forward(1, l + 1)
        if l + 2 < layers:
            for kind in (0, 2, 1):
                launch(kind, l + 2)
        for s in range(seqs):
            second[s].wait_recv()
            if last:
                out[s] = (hf[s, q].astype(F32) + r2[s, 0].astype(F32)).astype(BF16)
            else:
                nxt[s, h] = (hf[s].astype(F32) + r2[s].astype(F32)).astype(BF16)
                third.append(stage(2, s, nxt.at[s, h], nxt.at[s, h], core_peer))
        gathers = third
        if not last:
            arrived(0, l + 1)

    pl.when(has_right)(to_right.wait_send)
    pl.when(has_left)(to_left.wait_send)
    for c in pending:
        c.wait_send()


def body(activations, norm_gain, in_weight, out_weight, mixing, pool_scale):
    sp_size, tp_size = lax.axis_size("sp"), lax.axis_size("tp")
    layers, in_rows, cols = in_weight.shape
    seqs, toks, blk = activations.shape
    groups = mixing.shape[1] * tp_size
    halo = 2 ** (groups - 1)
    assert tp_size == 4 and mixing.shape[1] == 1 and sp_size % 4 == 0 and layers * halo <= toks
    mixing = mixing.reshape(layers, mixing.shape[2], mixing.shape[3])
    major = sp_size // MINOR
    n0 = toks + 2 * layers * halo
    scratch = [
        pltpu.VMEM(activations.shape, BF16),
        pltpu.VMEM(norm_gain.shape, F32),
        pltpu.VMEM(pool_scale.shape, F32),
        pltpu.VMEM((layers, sp_size, in_rows, cols), BF16),
        pltpu.VMEM((layers, sp_size) + out_weight.shape[1:], BF16),
        pltpu.VMEM((layers, sp_size) + mixing.shape[1:], BF16),
        pltpu.VMEM((2, 2, seqs, n0, blk), BF16),
    ]
    for l in range(layers):
        n = n0 - 2 * (l + 1) * halo
        scratch += [
            pltpu.VMEM((seqs, 2, 2, n, blk), BF16),
            pltpu.VMEM((seqs, 2, n, blk), BF16),
            pltpu.VMEM((seqs, 2, n, blk), BF16),
            pltpu.VMEM((seqs, 2, n, blk), BF16),
            pltpu.VMEM((seqs, 2, 2, n, blk), BF16),
        ]
    dma = pltpu.SemaphoreType.DMA
    scratch += [
        dma((3, layers, major)), dma((3, layers, major)),
        dma((3, layers, major)), dma((3, layers, major)),
        dma((6,)), dma((3, 4)), dma((3, 4)), dma((3, layers, seqs)), dma((3, layers, seqs)),
    ]
    return pl.pallas_call(
        functools.partial(kernel, sp_size, halo),
        out_shape=jax.ShapeDtypeStruct(activations.shape, BF16),
        in_specs=[pl.BlockSpec(memory_space=pl.ANY)] * 6,
        out_specs=pl.BlockSpec(memory_space=pltpu.VMEM),
        scratch_shapes=scratch,
        compiler_params=pltpu.CompilerParams(collective_id=0, has_side_effects=True),
    )(activations, norm_gain, in_weight, out_weight, mixing, pool_scale)


def solution(mesh):
    return jax.shard_map(
        body,
        mesh=mesh,
        in_specs=(
            P(None, "sp", "tp"),
            P(),
            P(None, "sp", "tp"),
            P(None, "tp", "sp"),
            P(None, "tp", "sp", None),
            P(None, "tp"),
        ),
        out_specs=P(None, "sp", "tp"),
        check_vma=False,
    )
```

profile of v0, /device:TPU:0, one launch (start us, length us, event | category | flops | bytes accessed | tf_op | source)
XLA Modules:
  0.0 78.0 jit_solution(9152727186373690358)
XLA Ops:
  0.0 1.5 %copy.7.w_out = bf16[4,128,32]{2,1,0:T(8,128)(2,1)} copy(bf16[4,128,32]{1,2,0:T(8,128)(2,1)} %param.9) | data formatting | bytes 65536 | tf_op args[3]
  1.5 75.1 %shard_map.64 = bf16[2,32,256]{2,1,0:T(8,128)(2,1)} custom-call(bf16[2,32,256]{2,1,0:T(8,128)(2,1)} %act_in.1, f32[4,1024]{1,0:T(4,128)} %gain_in.1, bf16[4,32,128]{2,1,0:T(8,128)(2,1)} %w_in.1, bf16[4,128,32]{2,1,0:T(8,128)(2,1)} %copy.7.w_out, bf16[4,4,128]{2,1,0:T(4,128)(2,1)} %bitcast.1, f32[4,128]{1,0:T(4,128)} %scale_in.1), custom_call_target="tpu_custom_call" | custom-call | tf_op jit(solution)/shard_map/pallas_call | solution.py:288
  76.6 1.4 %copy.9 = bf16[2,32,256]{2,1,0:T(8,128)(2,1)} copy(bf16[2,32,256]{2,1,0:T(8,128)(2,1)} %shard_map.64) | data formatting | bytes 65536
where the time goes:
time: 78.3 us; the launch traced here: 78 us
  Pallas kernels  75.1 us (96%)
  local copies, waits for them, and re-layouts  2.87 us (4%)
    pallas_call x1, Pallas kernels, body(): pl.pallas_call(functools.partial(kernel, sp_size, halo), out_shape=jax.Sh...  75.1 us
    unnamed x2, local copies, waits for them, and re-layouts  2.87 us

commit v1 on v0

v1 whole, which is shorter than its diff:
```python
import functools

import jax
import jax.numpy as jnp
from jax import lax
from jax.experimental import pallas as pl
from jax.experimental.pallas import tpu as pltpu
from jax.sharding import PartitionSpec as P

F32, BF16 = jnp.float32, jnp.bfloat16
RING = 4
HALO = 8
MIX = 8
ORDERS = ("xyz", "yzx", "zxy", "xyz", "yzx", "zxy", "xyz", "yzx", "zxy")
ROUNDS = ((0, 1, 8, 2), (3, 4, 5), (6, 7))


def kernel(
    act_in, gain_in, w_in, w_out, mix, scale_in, out,
    act, gain, scale, raw, gw, gm, x0, st1, st2, st3, fin, fo,
    s_own, r1, r2, r3, rd, s1, s2, s3, sd, s_act, r_act, s_sc, r_sc, s_h, r_h, s_f, r_f,
):
    layers = gain.shape[0]
    seqs, toks, blk = act.shape
    width = gain.shape[1]
    sp, tp = lax.axis_index("sp"), lax.axis_index("tp")
    sp_size = lax.axis_size("sp")
    c = sp % 2
    me = {"x": tp, "y": (sp // 2) % RING, "z": sp // (2 * RING)}
    seq, half = tp // 2, tp % 2
    seq_len = toks * sp_size
    n0 = x0.shape[1] - 16

    def off(axis, k):
        return lax.rem(me[axis] + (k % RING), RING)

    def device(axis=None, k=0, core=None):
        p = dict(me)
        if axis is not None:
            p[axis] = off(axis, k)
        cc = c if core is None else core
        return {"sp": (p["z"] * RING + p["y"]) * 2 + cc, "tp": p["x"]}

    def near(k):
        return {"sp": lax.rem(sp + k + sp_size, sp_size), "tp": tp}

    partner = device(core=1 - c)

    def remote(src, dst, ss, rs, to):
        return pltpu.make_async_remote_copy(
            src_ref=src, dst_ref=dst, send_sem=ss, recv_sem=rs, device_id=to, device_id_type=pl.DeviceIdType.MESH
        )

    def block(u, sel, r=None, core=None):
        ix = tuple(sel.get(a, slice(None)) for a in "xzy") + (c if core is None else core,)
        if r is not None:
            ix += (r,)
        return gm.at[ix] if u == MIX else gw.at[(u,) + ix]

    def send(ref, ss, rs, to):
        remote(ref, ref, ss, rs, to).start()

    def arrive(ref, rs):
        remote(ref, ref, rs, rs, partner).wait_recv()

    loads = []
    for l in range(layers):
        loads.append(pltpu.make_async_copy(w_in.at[l], gw.at[2 * l, tp, me["z"], me["y"], c], s_own.at[l]))
    loads.append(pltpu.make_async_copy(mix, gm.at[tp, me["z"], me["y"], c], s_own.at[4]))
    loads.append(pltpu.make_async_copy(w_out, raw, s_own.at[5]))
    loads.append(pltpu.make_async_copy(act_in, act, s_own.at[6]))
    loads.append(pltpu.make_async_copy(act_in.at[seq], x0.at[tp, pl.ds(toks, toks)], s_own.at[7]))
    loads.append(pltpu.make_async_copy(scale_in, scale.at[tp], s_own.at[8]))
    loads.append(pltpu.make_async_copy(gain_in, gain, s_own.at[9]))

    barrier = pltpu.get_barrier_semaphore()
    chip_next = {"sp": lax.rem(sp + jnp.where(c == 0, -1, 1) + sp_size, sp_size), "tp": tp}
    everyone = [partner, chip_next] + [device("x", k) for k in (1, 2, 3)]
    everyone += [device(a, k) for a in "yz" for k in (1, 2, 3)]
    for d in everyone:
        pl.semaphore_signal(barrier, inc=1, device_id=d, device_id_type=pl.DeviceIdType.MESH)
    for copy in loads:
        copy.start()
    for copy in loads[:5]:
        copy.wait()
    pl.semaphore_wait(barrier, len(everyone))

    mine = {a: me[a] for a in "xyz"}

    def p1(u):
        a1 = ORDERS[u][0]
        for k in (2, 1, 3):
            send(block(u, mine), s1.at[u], r1.at[u, (-k) % RING], device(a1, k))

    def p1_wait(u):
        a1 = ORDERS[u][0]
        for m in (1, 3, 2):
            arrive(block(u, {**mine, a1: off(a1, m)}), r1.at[u, m])

    def p2(u):
        p1_wait(u)
        a1, a2, a3 = ORDERS[u]
        line = block(u, {a2: me[a2], a3: me[a3]})
        send(line, s2.at[u], r2.at[u, 3], device(a2, 1))
        send(line, s2.at[u], r2.at[u, 1], device(a2, -1))

    def p2_forward(u):
        a1, a2, a3 = ORDERS[u]
        arrive(block(u, {a2: off(a2, 1), a3: me[a3]}), r2.at[u, 1])
        send(block(u, {a2: off(a2, 1), a3: me[a3]}, r=0), s2.at[u], r2.at[u, 2], device(a2, -1))
        arrive(block(u, {a2: off(a2, 3), a3: me[a3]}), r2.at[u, 3])
        send(block(u, {a2: off(a2, 3), a3: me[a3]}, r=1), s2.at[u], r2.at[u, 0], device(a2, 1))

    def p2_opposite(u):
        a1, a2, a3 = ORDERS[u]
        arrive(block(u, {a2: off(a2, 2), a3: me[a3]}, r=0), r2.at[u, 2])
        arrive(block(u, {a2: off(a2, 2), a3: me[a3]}, r=1), r2.at[u, 0])

    def p3(u, j):
        a1, a2, a3 = ORDERS[u]
        ref = block(u, {a2: off(a2, j), a3: me[a3]})
        send(ref, s3.at[u], r3.at[u, j, 3], device(a3, 1))
        send(ref, s3.at[u], r3.at[u, j, 1], device(a3, -1))

    def p3_forward(u, j):
        a1, a2, a3 = ORDERS[u]
        arrive(block(u, {a2: off(a2, j), a3: off(a3, 1)}), r3.at[u, j, 1])
        send(block(u, {a2: off(a2, j), a3: off(a3, 1)}, r=0), s3.at[u], r3.at[u, j, 2], device(a3, -1))
        arrive(block(u, {a2: off(a2, j), a3: off(a3, 3)}), r3.at[u, j, 3])
        send(block(u, {a2: off(a2, j), a3: off(a3, 3)}, r=1), s3.at[u], r3.at[u, j, 0], device(a3, 1))

    def p3_opposite(u):
        a1, a2, a3 = ORDERS[u]
        for j in range(RING):
            arrive(block(u, {a2: off(a2, j), a3: off(a3, 2)}, r=0), r3.at[u, j, 2])
            arrive(block(u, {a2: off(a2, j), a3: off(a3, 2)}, r=1), r3.at[u, j, 0])

    def d2d(u, k):
        a3 = ORDERS[u][2]
        send(block(u, {a3: off(a3, k)}), sd.at[u], rd.at[u], partner)

    def d2d_wait(u):
        arrive(block(u, {}, core=1 - c), rd.at[u])

    def finish_sends(u):
        zero = {"z": 0, "y": 0}
        three = pl.ds(0, 3)
        for ref, sem in (
            (block(u, {**zero, "x": three}), s1), (block(u, {"z": 0, "x": three}), s2),
            (block(u, {"x": three}), s3), (block(u, {}), sd),
        ):
            remote(ref, ref, sem.at[u], sem.at[u], partner).wait_send()

    for u in (0, 8, 2, 4, 6):
        p1(u)
    loads[5].wait()
    for l in range(layers):
        t = raw[l].astype(F32).T.astype(BF16).reshape(2, 16, 128)
        gw[2 * l + 1, tp, me["z"], me["y"], c] = t
    for u in (1, 3, 5, 7):
        p1(u)
    for copy in loads[6:]:
        copy.wait()
    spread = []
    for k in (2, 1, 3):
        t_to = off("x", k)
        m = (-k) % RING
        spread.append(
            remote(act.at[t_to // 2], x0.at[tp, pl.ds(toks, toks)], s_act.at[k], r_act.at[m], device("x", k))
        )
        spread.append(remote(scale.at[tp], scale.at[tp], s_sc.at[k], r_sc.at[m], device("x", k)))
    for copy in spread:
        copy.start()

    has_left, has_right = sp > 0, sp < sp_size - 1
    rows = lambda i: x0.at[:, pl.ds(i * toks, toks)]
    to_right = remote(rows(1), rows(0), s_h.at[0], r_h.at[0], near(1))
    to_left = remote(rows(1), rows(2), s_h.at[1], r_h.at[1], near(-1))

    def blank(i):
        def fill():
            x0[:, i * toks : (i + 1) * toks, :] = jnp.zeros((RING, toks, blk), BF16)

        return fill

    pl.when(jnp.logical_not(has_left))(blank(0))
    pl.when(jnp.logical_not(has_right))(blank(2))

    def halo():
        for m in (1, 3, 2):
            arrive(x0.at[off("x", m), pl.ds(toks, toks)], r_act.at[m])
            arrive(scale.at[off("x", m)], r_sc.at[m])
        pl.when(has_right)(to_right.start)
        pl.when(has_left)(to_left.start)

    def halo_wait():
        pl.when(has_left)(to_right.wait_recv)
        pl.when(has_right)(to_left.wait_recv)

    states = [None, st1, st2, st3]

    def load_rows(l, t):
        n = n0 - 2 * HALO * l
        if l == 0:
            return x0[t, pl.ds(pl.multiple_of(16 * half, 16), n), :]
        return states[l][t]

    def project(l):
        xs = [load_rows(l, t).astype(F32) for t in range(RING)]
        total = sum(jnp.sum(x * x, axis=-1, keepdims=True) for x in xs)
        inv = lax.rsqrt(total * (1.0 / width) + 1e-06)
        normed = jnp.concatenate(
            [(xs[t] * inv * gain[l : l + 1, t * blk : (t + 1) * blk]).astype(BF16) for t in range(RING)], axis=1
        )
        pooled = []
        for p in range(2):
            w = jnp.concatenate([gw[2 * l, 2 * p + i].reshape(width, 128) for i in range(2)], axis=1)
            pooled.append(jnp.dot(normed, w, preferred_element_type=F32).astype(BF16))
        return pooled

    def mixed(l, pooled):
        n_in = n0 - 2 * HALO * l
        n_out = n_in - 2 * HALO
        base = sp * toks + 16 * half - 4 * HALO + HALO * l
        parts = []
        for g in range(RING):
            reach = 2**g
            pos = base + HALO + lax.broadcasted_iota(jnp.int32, (n_out, n_in), 0)
            src = base + lax.broadcasted_iota(jnp.int32, (n_out, n_in), 1)
            low = jnp.maximum(pos - reach, 0)
            high = jnp.minimum(pos + reach, seq_len)
            band = jnp.where((src >= low) & (src < high), 1.0, 0.0).astype(BF16)
            col = base + HALO + lax.broadcasted_iota(jnp.int32, (n_out, 1), 0)
            count = jnp.minimum(col + reach, seq_len) - jnp.maximum(col - reach, 0)
            inv_count = 1.0 / jnp.maximum(count, 1).astype(F32)
            values = pooled[g // 2][:, (g % 2) * 128 : (g % 2 + 1) * 128]
            sums = jnp.dot(band, values, preferred_element_type=F32)
            centred = (sums * inv_count - values.astype(F32)[HALO : HALO + n_out]).astype(BF16)
            m = gm[g, :, :, :, l // 2, l % 2].astype(F32).reshape(128, 128).astype(BF16)
            y = jnp.dot(centred, m, preferred_element_type=F32)
            parts.append((y * scale[g, l : l + 1, :]).astype(BF16))
        return jnp.concatenate(parts, axis=1)

    def out_block(l, joined, q):
        w = jnp.concatenate([gw[2 * l + 1, t, q].reshape(blk, 128) for t in range(RING)], axis=1)
        return lax.dot_general(joined, w, (((1,), (1,)), ((), ())), preferred_element_type=F32).astype(BF16)

    def expand(l, joined):
        for q in range(RING):
            states[l + 1][q] = out_block(l, joined, q)

    r_first, r_second, r_third = ROUNDS
    later = r_second + r_third
    for u in r_first:
        p2(u)
        p3(u, 0)
    halo()
    for u in r_second:
        p2(u)
    for u in r_first:
        p2_forward(u)
        p3(u, 1)
        p3(u, 3)
    for u in r_third:
        p2(u)
    for u in r_first:
        p2_opposite(u)
        p3(u, 2)
        d2d(u, 0)
    for u in r_second:
        p2_forward(u)
    for j in (0, 1, 3):
        for u in r_first:
            p3_forward(u, j)
    for u in r_third:
        p2_forward(u)
    for u in r_first:
        p3_forward(u, 2)
        d2d(u, 1)
        d2d(u, 3)
    for u in r_second:
        p2_opposite(u)
        for j in range(RING):
            p3(u, j)
        d2d(u, 0)
    for u in r_first:
        p3_opposite(u)
        d2d(u, 2)
    for u in r_third:
        p2_opposite(u)
        d2d(u, 0)
    halo_wait()
    d2d_wait(0)
    pooled = project(0)
    d2d_wait(8)
    joined = mixed(0, pooled)
    d2d_wait(1)
    expand(0, joined)
    for u in r_second:
        for j in range(RING):
            p3_forward(u, j)
        d2d(u, 1)
        d2d(u, 3)
    for u in r_third:
        for j in range(RING):
            p3(u, j)
    d2d_wait(2)
    pooled = project(1)
    joined = mixed(1, pooled)
    for u in r_second:
        p3_opposite(u)
        d2d(u, 2)
    d2d_wait(3)
    expand(1, joined)
    for u in r_third:
        for j in range(RING):
            p3_forward(u, j)
        d2d(u, 1)
        d2d(u, 3)
    d2d_wait(4)
    pooled = project(2)
    joined = mixed(2, pooled)
    d2d_wait(5)
    expand(2, joined)
    for u in r_third:
        p3_opposite(u)
        d2d(u, 2)
    d2d_wait(6)
    pooled = project(3)
    joined = mixed(3, pooled)
    d2d_wait(7)
    final = []
    for k in (2, 1, 3, 0):
        q = off("x", k)
        fin[q] = out_block(3, joined, q)
        if k:
            copy = remote(fin.at[q], fo.at[tp], s_f.at[k], r_f.at[(-k) % RING], device("x", k))
            copy.start()
            final.append(copy)
    for u in range(9):
        finish_sends(u)
    for copy in spread:
        copy.wait_send()
    pl.when(has_right)(to_right.wait_send)
    pl.when(has_left)(to_left.wait_send)
    fo[tp] = fin[tp]
    for m in (1, 3, 2):
        arrive(fo.at[off("x", m)], r_f.at[m])
    for s in range(seqs):
        for i in range(2):
            out[s, 16 * i : 16 * (i + 1), :] = fo[2 * s + i]
    for copy in final:
        copy.wait_send()


def body(activations, norm_gain, in_weight, out_weight, mixing, pool_scale):
    layers, in_rows, cols = in_weight.shape
    seqs, toks, blk = activations.shape
    tp_size = lax.axis_size("tp")
    assert (layers, in_rows, cols, seqs, toks, blk, tp_size) == (4, 32, 128, 2, 32, 256, RING)
    in_weight = in_weight.reshape(layers, 2, 16, cols)
    mixing = mixing.reshape(2, 2, 4, cols)
    dma = pltpu.SemaphoreType.DMA
    zs = lax.axis_size("sp") // (2 * RING)
    n0 = toks + 2 * toks
    scratch = [
        pltpu.VMEM(activations.shape, BF16),
        pltpu.VMEM(norm_gain.shape, F32),
        pltpu.VMEM((RING, layers, cols), F32),
        pltpu.VMEM(out_weight.shape, BF16),
        pltpu.VMEM((8, RING, zs, RING, 2, 2, 16, cols), BF16),
        pltpu.VMEM((RING, zs, RING, 2, 2, 2, 4, cols), BF16),
        pltpu.VMEM((RING, n0, blk), BF16),
        pltpu.VMEM((RING, 64, blk), BF16),
        pltpu.VMEM((RING, 48, blk), BF16),
        pltpu.VMEM((RING, 32, blk), BF16),
        pltpu.VMEM((RING, 16, blk), BF16),
        pltpu.VMEM((RING, 16, blk), BF16),
        dma((10,)),
        dma((9, RING)), dma((9, RING)), dma((9, RING, RING)), dma((9,)),
        dma((9,)), dma((9,)), dma((9,)), dma((9,)),
        dma((4,)), dma((4,)), dma((4,)), dma((4,)), dma((2,)), dma((2,)), dma((4,)), dma((4,)),
    ]
    return pl.pallas_call(
        kernel,
        out_shape=jax.ShapeDtypeStruct(activations.shape, BF16),
        in_specs=[pl.BlockSpec(memory_space=pl.ANY)] * 6,
        out_specs=pl.BlockSpec(memory_space=pltpu.VMEM),
        scratch_shapes=scratch,
        compiler_params=pltpu.CompilerParams(collective_id=0, has_side_effects=True),
    )(activations, norm_gain, in_weight, out_weight, mixing, pool_scale)


def solution(mesh):
    return jax.shard_map(
        body,
        mesh=mesh,
        in_specs=(
            P(None, "sp", "tp"),
            P(),
            P(None, "sp", "tp"),
            P(None, "tp", "sp"),
            P(None, "tp", "sp", None),
            P(None, "tp"),
        ),
        out_specs=P(None, "sp", "tp"),
        check_vma=False,
    )
```

time: 78.3 us -> 51 us (0.65)
  the two profiles are of different devices: /device:TPU:0 before, /device:TPU:1 now
where the time goes in v1:
time: 51 us; the launch traced here: 50.7 us
  Pallas kernels  47.8 us (94%)
  local copies, waits for them, and re-layouts  2.87 us (6%)
    pallas_call x1, Pallas kernels, body(): pl.pallas_call(kernel, out_shape=jax.ShapeDtypeStruct(activations.shape,...  47.8 us
    unnamed x2, local copies, waits for them, and re-layouts  2.87 us

profile of v1, /device:TPU:1, one launch (start us, length us, event | category | flops | bytes accessed | tf_op | source)
XLA Modules:
  0.0 50.7 jit_solution(18053631912683244329)
XLA Ops:
  0.0 1.5 %copy.7.w_out = bf16[4,128,32]{2,1,0:T(8,128)(2,1)} copy(bf16[4,128,32]{1,2,0:T(8,128)(2,1)} %param.9) | data formatting | bytes 65536 | tf_op args[3]
  1.5 47.8 %shard_map.64 = bf16[2,32,256]{2,1,0:T(8,128)(2,1)} custom-call(bf16[2,32,256]{2,1,0:T(8,128)(2,1)} %act_in.1, f32[4,1024]{1,0:T(4,128)} %gain_in.1, bf16[4,2,16,128]{3,2,1,0:T(8,128)(2,1)} %bitcast.2, bf16[4,128,32]{2,1,0:T(8,128)(2,1)} %copy.7.w_out, bf16[2,2,4,128]{3,2,1,0:T(4,128)(2,1)} %bitcast.3, f32[4,128]{1,0:T(4,128)} %scale_in.1), custom_call_target="tpu_custom_call" | custom-call | tf_op jit(solution)/shard_map/pallas_call | solution.py:384
  49.3 1.4 %copy.9 = bf16[2,32,256]{2,1,0:T(8,128)(2,1)} copy(bf16[2,32,256]{2,1,0:T(8,128)(2,1)} %shard_map.64) | data formatting | bytes 65536
